TPU v7x, 32 devices: a whole 2x2x4 slice. The times are simulated.
32 devices in a mesh: fs: 16 (over z, y, x), tp: 2 (over core).
Axes of the slice: x: 2, y: 2, z: 4, core: 2. Of those that a mesh axis runs over, the one named last changes fastest.
Arguments:
- tokens: bfloat16 [2, 256, 2048], P('tp'), may hold values from -6 to 6
- gain_first: float32 [2048], P('fs'), may hold values from 0.1 to 1.9
- gate_first: float32 [2048, 5632], P('fs', 'tp'), may hold values from -0.125 to 0.125
- up_first: float32 [2048, 5632], P('fs', 'tp'), may hold values from -0.125 to 0.125
- down_first: float32 [2048, 5632], P('fs', 'tp'), may hold values from -0.3125 to 0.3125
- gain_second: float32 [2048], P('fs'), may hold values from 0.1 to 1.9
- gate_second: float32 [2048, 5632], P('fs', 'tp'), may hold values from -0.125 to 0.125
- up_second: float32 [2048, 5632], P('fs', 'tp'), may hold values from -0.125 to 0.125
- down_second: float32 [2048, 5632], P('fs', 'tp'), may hold values from -0.3125 to 0.3125
Outputs:
- mixed: bfloat16 [2, 256, 2048], P('tp', 'fs')
- served_gate_first: bfloat16 [2, 2816, 2048], P(None, 'fs')
- served_up_first: bfloat16 [2, 2816, 2048], P(None, 'fs')
- served_down_first: bfloat16 [2, 2816, 2048], P(None, 'fs')
- served_gate_second: bfloat16 [2, 2816, 2048], P(None, 'fs')
- served_up_second: bfloat16 [2, 2816, 2048], P(None, 'fs')
- served_down_second: bfloat16 [2, 2816, 2048], P(None, 'fs')
All inputs are finite; a program needn't handle non-finite values.
Results may differ from a plain program's by a relative error of at most 0.013.
Values may be sent and summed in bfloat16 or wider, within the bound.
A program may use at most 64 MiB of HBM per device.

v0:
```python
import jax
import jax.numpy as jnp
from jax import lax
from jax.sharding import PartitionSpec as P


def normalize(values):
    wide = values.astype(jnp.float32)
    scale = lax.rsqrt(jnp.mean(wide * wide, axis=-1, keepdims=True) + 1e-06)
    return (wide * scale).astype(jnp.bfloat16)


def folded(weight, gain):
    return (weight * gain[:, None]).astype(jnp.bfloat16).T


def relayout(gate_part, up_part, down_part):
    gate_cut, up_cut, down_cut = (
        lax.all_to_all(gate_part, "fs", split_axis=0, concat_axis=1, tiled=True),
        lax.all_to_all(up_part, "fs", split_axis=0, concat_axis=1, tiled=True),
        lax.all_to_all(down_part, "fs", split_axis=0, concat_axis=1, tiled=True),
    )
    return (
        lax.all_gather(gate_cut[None], "tp", axis=0, tiled=True),
        lax.all_gather(up_cut[None], "tp", axis=0, tiled=True),
        lax.all_gather(down_cut[None], "tp", axis=0, tiled=True),
    )


def hidden_of(normed, gate_served, up_served):
    gate_flat = gate_served.reshape(-1, gate_served.shape[2])
    up_flat = up_served.reshape(-1, up_served.shape[2])
    gate_act = jnp.einsum("rd,hd->rh", normed, gate_flat, preferred_element_type=jnp.float32)
    up_act = jnp.einsum("rd,hd->rh", normed, up_flat, preferred_element_type=jnp.float32)
    return (jax.nn.silu(gate_act) * up_act).astype(jnp.bfloat16)


def projector(hidden, down_flat):
    return jnp.dot(hidden, down_flat, preferred_element_type=jnp.float32)


def shards(
    tokens,
    gain_first,
    gate_first,
    up_first,
    down_first,
    gain_second,
    gate_second,
    up_second,
    down_second,
):
    gate_one, up_one, down_one = relayout(
        folded(gate_first, gain_first),
        folded(up_first, gain_first),
        down_first.astype(jnp.bfloat16).T,
    )
    gate_two, up_two, down_two = relayout(
        folded(gate_second, gain_second),
        folded(up_second, gain_second),
        down_second.astype(jnp.bfloat16).T,
    )
    rows = tokens[0]
    keep = rows.shape[0] // lax.axis_size("fs")
    offset = lax.axis_index("fs") * keep
    hidden_first = hidden_of(normalize(rows), gate_one, up_one)
    down_flat_one = down_one.reshape(-1, down_one.shape[2])
    partial_value = jnp.dot(hidden_first, down_flat_one, preferred_element_type=jnp.float32)
    branch = lax.psum(partial_value, "fs")
    whole_middle = (rows.astype(jnp.float32) + 0.5 * branch).astype(jnp.bfloat16)
    hidden_second = hidden_of(normalize(whole_middle), gate_two, up_two)
    middle = lax.dynamic_slice_in_dim(whole_middle, offset, keep, 0)
    down_flat_two = down_two.reshape(-1, down_two.shape[2])
    branch_two = lax.psum_scatter(
        projector(hidden_second, down_flat_two), "fs", scatter_dimension=0, tiled=True
    )
    mixed = (middle.astype(jnp.float32) + 0.5 * branch_two).astype(jnp.bfloat16)[None]
    return (mixed, gate_one, up_one, down_one, gate_two, up_two, down_two)


def solution(mesh):
    return jax.shard_map(
        shards,
        mesh=mesh,
        in_specs=(
            P("tp", None, None),
            P("fs"),
            P("fs", "tp"),
            P("fs", "tp"),
            P("fs", "tp"),
            P("fs"),
            P("fs", "tp"),
            P("fs", "tp"),
            P("fs", "tp"),
        ),
        out_specs=(
            P("tp", "fs", None),
            P(None, "fs", None),
            P(None, "fs", None),
            P(None, "fs", None),
            P(None, "fs", None),
            P(None, "fs", None),
            P(None, "fs", None),
        ),
        check_vma=False,
    )
```

profile of v0, /device:TPU:0, one launch (start us, length us, event | category | flops | bytes accessed | tf_op | source)
XLA Modules:
  0.0 395.1 jit_solution(5311903597791260053)
XLA Ops:
  7.2 1.8 copy.40
  9.0 1.8 copy.42
  10.8 1.1 multiply_convert_fusion.3
  11.9 28.1 %all_to_all.96 = bf16[16,176,128]{2,1,0:T(8,128)(2,1)S(1)} all-to-all(bf16[16,176,128]{2,1,0:T(8,128)(2,1)S(1)} %bitcast.56), channel_id=1, replica_groups=mesh['fs'=16,'tp'=2] {'fs'}, dimensions={0} | all-to-all | bytes 1441792 | tf_op jit(solution)/shard_map/all_to_all | solution.py:19
  40.3 1.2 broadcast_in_dim.27
  41.5 22.3 %all_to_all.97 = bf16[16,176,128]{2,1,0:T(8,128)(2,1)S(1)} all-to-all(bf16[16,176,128]{2,1,0:T(8,128)(2,1)S(1)} %bitcast.54), channel_id=1, replica_groups=mesh['fs'=16,'tp'=2] {'fs'}, dimensions={0} | all-to-all | bytes 1441792 | tf_op jit(solution)/shard_map/all_to_all | solution.py:20
  64.0 1.2 broadcast_in_dim.28
  65.3 0.4 copy-done.3
  65.7 0.4 copy.44
  66.0 22.3 %all_to_all.98 = bf16[16,176,128]{2,1,0:T(8,128)(2,1)S(1)} all-to-all(bf16[16,176,128]{2,1,0:T(8,128)(2,1)S(1)} %bitcast.64), channel_id=1, replica_groups=mesh['fs'=16,'tp'=2] {'fs'}, dimensions={0} | all-to-all | bytes 1441792 | tf_op jit(solution)/shard_map/all_to_all | solution.py:21
  88.5 1.2 broadcast_in_dim.29
  89.8 0.4 copy-done.4
  90.1 0.4 copy.46
  90.6 1.8 copy.48
  92.4 1.6 fusion.4
  94.0 2.5 fusion.14
  96.5 0.6 all-gather.11.cloned.1.call-done
  97.1 5.5 %fusion.10 = f32[256,2048]{1,0:T(8,128)} fusion(bf16[352,2048]{1,0:T(8,128)(2,1)} %bitcast.68, bf16[352,2048]{1,0:T(8,128)(2,1)} %bitcast.67, bf16[1,256,2048]{2,1,0:T(8,128)(2,1)} %param.9, f32[256]{0:T(256)S(1)} %add_rsqrt_fusion.1, f32[256,352]{0,1:T(8,128)S(1)} %fusion.14), kind=kOutput, calls=%fused_computation.20 | convolution fusion | flops 740311040 | bytes 6390784 | tf_op jit(solution)/shard_map/dot_general | solution.py:68
  102.7 0.6 copy-done.13
  103.3 1.1 multiply_convert_fusion.1
  104.3 41.4 %all_to_all.99 = bf16[16,176,128]{2,1,0:T(8,128)(2,1)S(1)} all-to-all(bf16[16,176,128]{2,1,0:T(8,128)(2,1)S(1)} %bitcast.57), channel_id=1, replica_groups=mesh['fs'=16,'tp'=2] {'fs'}, dimensions={0} | all-to-all | bytes 1441792 | tf_op jit(solution)/shard_map/all_to_all | solution.py:19
  145.9 1.2 broadcast_in_dim.30
  147.2 26.7 %all_to_all.100 = bf16[16,176,128]{2,1,0:T(8,128)(2,1)S(1)} all-to-all(bf16[16,176,128]{2,1,0:T(8,128)(2,1)S(1)} %bitcast.55), channel_id=1, replica_groups=mesh['fs'=16,'tp'=2] {'fs'}, dimensions={0} | all-to-all | bytes 1441792 | tf_op jit(solution)/shard_map/all_to_all | solution.py:20
  174.1 1.2 broadcast_in_dim.31
  175.3 0.4 copy-done.5
  175.7 0.3 copy.50
  176.0 23.5 %all_to_all.101 = bf16[16,176,128]{2,1,0:T(8,128)(2,1)S(1)} all-to-all(bf16[16,176,128]{2,1,0:T(8,128)(2,1)S(1)} %bitcast.65), channel_id=1, replica_groups=mesh['fs'=16,'tp'=2] {'fs'}, dimensions={0} | all-to-all | bytes 1441792 | tf_op jit(solution)/shard_map/all_to_all | solution.py:21
  199.7 1.2 broadcast_in_dim.32
  201.2 50.3 %all-reduce.2.cloned.1.call-done = f32[256,2048]{1,0:T(8,128)} async-done(((f32[256,2048]{1,0:T(8,128)}), f32[256,2048]{1,0:T(8,128)}) %all-reduce.2.cloned.1.call-update) | async-done | bytes 2097168 | tf_op jit(solution)/shard_map/psum | solution.py:69
  251.4 2.1 fusion.2
  253.6 8.7 %all-gather.13.cloned.1.call-done = bf16[2,176,2048]{2,1,0:T(8,128)(2,1)} async-done(((bf16[1,176,2048]{2,1,0:T(8,128)(2,1)}), bf16[2,176,2048]{2,1,0:T(8,128)(2,1)}) %all-gather.13.cloned.1.call-update) | async-done | bytes 1441808 | tf_op jit(solution)/shard_map/all_gather | solution.py:24
  262.3 2.0 fusion.18
  264.3 10.8 %all-gather.15.cloned.1.call-done = bf16[2,176,2048]{2,1,0:T(8,128)(2,1)} async-done(((bf16[1,176,2048]{2,1,0:T(8,128)(2,1)}), bf16[2,176,2048]{2,1,0:T(8,128)(2,1)}) %all-gather.15.cloned.1.call-update) | async-done | bytes 1441808 | tf_op jit(solution)/shard_map/all_gather | solution.py:25
  275.1 12.9 %all-gather.17.cloned.1.call-done = bf16[2,176,2048]{2,1,0:T(8,128)(2,1)} async-done(((bf16[1,176,2048]{2,1,0:T(8,128)(2,1)}), bf16[2,176,2048]{2,1,0:T(8,128)(2,1)}) %all-gather.17.cloned.1.call-update) | async-done | bytes 1441808 | tf_op jit(solution)/shard_map/all_gather | solution.py:26
  288.0 5.2 %fusion.9 = f32[256,2048]{1,0:T(8,128)} fusion(bf16[352,2048]{1,0:T(8,128)(2,1)} %bitcast.71, bf16[352,2048]{1,0:T(8,128)(2,1)} %bitcast.70, bf16[256,2048]{1,0:T(8,128)(2,1)S(1)} %get-tuple-element.8, f32[256]{0:T(256)S(1)} %add_rsqrt_fusion, f32[256,352]{0,1:T(8,128)S(1)} %fusion.18), kind=kOutput, calls=%fused_computation.19 | convolution fusion | flops 740311040 | bytes 6390784 | tf_op jit(solution)/shard_map/dot_general | solution.py:39
  293.3 82.9 %reduce-scatter.2.cloned.1.call-done = f32[16,2048]{1,0:T(8,128)} async-done(((f32[256,2048]{1,0:T(8,128)}), f32[16,2048]{1,0:T(8,128)}) %reduce-scatter.2.cloned.1.call-update) | async-done | bytes 131088 | tf_op jit(solution)/shard_map/reduce_scatter | solution.py:74
  376.2 1.6 fusion.32
  377.7 1.1 copy.59
  378.8 0.8 copy-done.7
  379.6 1.1 copy.60
  380.7 0.8 copy-done.8
  381.5 1.1 copy.61
  382.6 0.8 copy-done.9
  383.4 1.1 copy.62
  384.5 0.8 copy-done.10
  385.3 1.1 copy.63
  386.4 0.8 copy-done.11
  387.1 1.1 copy.64
  (45 shorter events, 1.9 us)
Async XLA Ops:
  7.2 86.8 %all-gather.7.cloned.1.call-start = ((), (), s32[]{:S(2)}) async-start(), calls=%async_computation.7 | async-start | bytes 2162688 | tf_op jit(solution)/shard_map/all_gather | solution.py:24
  9.0 1.8 copy-start.12
  40.2 1.3 copy-start.1
  41.4 55.1 %all-gather.9.cloned.1.call-start = ((), (), s32[]{:S(2)}) async-start(), calls=%async_computation.8 | async-start | bytes 2162688 | tf_op jit(solution)/shard_map/all_gather | solution.py:25
  64.0 1.6 copy-start.3
  65.2 31.9 %all-gather.11.cloned.1.call-start = ((), (), s32[]{:S(2)}) async-start(), calls=%async_computation.9 | async-start | bytes 2162688 | tf_op jit(solution)/shard_map/all_gather | solution.py:26
  88.5 1.6 copy-start.4
  89.7 161.7 %all-reduce.2.cloned.1.call-start = ((), (), s32[]{:S(2)}) async-start(), calls=%async_computation.10 | async-start | bytes 4194304 | tf_op jit(solution)/shard_map/psum | solution.py:69
  102.6 0.7 copy-start.13
  102.6 159.6 %all-gather.13.cloned.1.call-start = ((), (), s32[]{:S(2)}) async-start(), calls=%async_computation.11 | async-start | bytes 2162688 | tf_op jit(solution)/shard_map/all_gather | solution.py:24
  145.9 1.3 copy-start.2
  147.1 127.9 %all-gather.15.cloned.1.call-start = ((), (), s32[]{:S(2)}) async-start(), calls=%async_computation.12 | async-start | bytes 2162688 | tf_op jit(solution)/shard_map/all_gather | solution.py:25
  174.1 1.6 copy-start.5
  175.3 112.7 %all-gather.17.cloned.1.call-start = ((), (), s32[]{:S(2)}) async-start(), calls=%async_computation.13 | async-start | bytes 2162688 | tf_op jit(solution)/shard_map/all_gather | solution.py:26
  199.7 51.7 %copy-start = (bf16[1,256,2048]{2,1,0:T(8,128)(2,1)S(1)}, bf16[1,256,2048]{2,1,0:T(8,128)(2,1)}, u32[]{:S(2)}) copy-start(bf16[1,256,2048]{2,1,0:T(8,128)(2,1)} %param.9) | copy-start | bytes 3145732
  200.9 175.2 %reduce-scatter.2.cloned.1.call-start = ((), (), s32[]{:S(2)}) async-start(), calls=%async_computation.14 | async-start | bytes 2228224 | tf_op jit(solution)/shard_map/reduce_scatter | solution.py:74
  293.2 84.5 %copy-start.6 = (bf16[2,176,2048]{2,1,0:T(8,128)(2,1)S(1)}, bf16[2,176,2048]{2,1,0:T(8,128)(2,1)}, u32[]{:S(2)}) copy-start(bf16[2,176,2048]{2,1,0:T(8,128)(2,1)} %all-gather.7.cloned.1.call-done) | copy-start | bytes 4325380
  377.7 1.9 copy-start.7
  379.6 1.9 copy-start.8
  381.5 1.9 copy-start.9
  383.4 1.9 copy-start.10
  385.3 1.9 copy-start.11
Sparse Core Ops, SparseCore 0:
  41.6 7.2 all-gather.6
  65.3 7.2 all-gather.8
  89.8 7.2 all-gather.10
  102.8 148.6 all-reduce.1
  253.4 8.8 all-gather.12
  264.3 10.7 all-gather.14
  277.2 10.7 all-gather.16
  293.4 82.7 reduce-scatter.1
where the time goes:
time: 396 us; the launch traced here: 395 us
  waiting for transfers between devices  166 us (42%)
  blocking collectives  164 us (41%)
  local copies, waits for them, and re-layouts  26.9 us (7%)
  matrix products  15.3 us (4%)
  between operations  14.3 us (4%)
  other arithmetic  7.42 us (2%)
    reduce_scatter x1, waiting for transfers between devices, shards(): lax.psum_scatter(projector(hidden_second, down_flat_two), 'fs', scatter_d...  82.9 us
    all_to_all x2, blocking collectives, relayout(): lax.all_to_all(gate_part, 'fs', split_axis=0, concat_axis=1, tiled=True)  69.5 us
    psum x1, waiting for transfers between devices, shards(): branch = lax.psum(partial_value, 'fs')  50.3 us
    all_to_all x2, blocking collectives, relayout(): lax.all_to_all(up_part, 'fs', split_axis=0, concat_axis=1, tiled=True)  49 us
    all_to_all x2, blocking collectives, relayout(): lax.all_to_all(down_part, 'fs', split_axis=0, concat_axis=1, tiled=True)  45.8 us
    unnamed x40, local copies, waits for them, and re-layouts  18.8 us
    all_gather x2, waiting for transfers between devices, relayout(): lax.all_gather(down_cut[None], 'tp', axis=0, tiled=True)  13.5 us
    all_gather x2, waiting for transfers between devices, relayout(): lax.all_gather(up_cut[None], 'tp', axis=0, tiled=True)  10.8 us
  transfers between devices with their start and end apart: 8, of which 6 were waited for; matrix products, arithmetic and copies ran while one was open for 5% of the time, Pallas kernels for 0%

commit v1 on v0

--- a/solution.py
+++ b/solution.py
@@ -66,7 +66,11 @@
     hidden_first = hidden_of(normalize(rows), gate_one, up_one)
     down_flat_one = down_one.reshape(-1, down_one.shape[2])
     partial_value = jnp.dot(hidden_first, down_flat_one, preferred_element_type=jnp.float32)
-    branch = lax.psum(partial_value, "fs")
+    size = lax.axis_size("fs")
+    branch, far = (partial_value, 1)
+    while far < size:
+        branch = branch + lax.ppermute(branch, "fs", [(i, i ^ far) for i in range(size)])
+        far = 2 * far
     whole_middle = (rows.astype(jnp.float32) + 0.5 * branch).astype(jnp.bfloat16)
     hidden_second = hidden_of(normalize(whole_middle), gate_two, up_two)
     middle = lax.dynamic_slice_in_dim(whole_middle, offset, keep, 0)

time: 396 us -> 490 us (1.24)
  waiting for transfers between devices: 166 us -> 228 us
  starting transfers between devices: 0.51 us -> 17.2 us
  other arithmetic: 7.42 us -> 16 us
  blocking collectives: 164 us -> 172 us
    ppermute x0 -> x4, waiting for transfers between devices: none -> 131 us  [shards(): lax.ppermute(branch, 'fs', [(i, i ^ far) for i in range(size)])]
    all_to_all x2, blocking collectives: 45.8 us -> 121 us  [relayout(): lax.all_to_all(down_part, 'fs', split_axis=0, concat_axis=1, tiled=True)]
    psum x1 -> x0, waiting for transfers between devices: 50.3 us -> none  [shards(): branch = lax.psum(partial_value, 'fs')]
    all_to_all x2 -> x1, blocking collectives: 69.5 us -> 28.1 us  [relayout(): lax.all_to_all(gate_part, 'fs', split_axis=0, concat_axis=1, tiled=True)]
    all_to_all x2 -> x1, blocking collectives: 49 us -> 22.3 us  [relayout(): lax.all_to_all(up_part, 'fs', split_axis=0, concat_axis=1, tiled=True)]
    all_to_all x0 -> x2, starting transfers between devices: none -> 11.3 us  [the longest x1 5.7 us: relayout(): lax.all_to_all(up_part, 'fs', split_axis=0, concat_axis=1, tiled=True)]
    all_gather x2, waiting for transfers between devices: 10.8 us -> 0.04 us  [relayout(): lax.all_gather(up_cut[None], 'tp', axis=0, tiled=True)]
    all_gather x2, waiting for transfers between devices: 8.75 us -> 0.04 us  [relayout(): lax.all_gather(gate_cut[None], 'tp', axis=0, tiled=True)]
  transfers between devices with their start and end apart: 8 -> 13, of which waited for: 6 -> 7; matrix products, arithmetic and copies ran while one was open for 5% -> 6% of each run, Pallas kernels for 0% -> 0%
where the time goes in v1:
time: 490 us; the launch traced here: 489 us
  waiting for transfers between devices  228 us (47%)
  blocking collectives  172 us (35%)
  local copies, waits for them, and re-layouts  28.4 us (6%)
  starting transfers between devices  17.2 us (4%)
  other arithmetic  16 us (3%)
  between operations  14.4 us (3%)
  matrix products  13.2 us (3%)
    ppermute x4, waiting for transfers between devices, shards(): lax.ppermute(branch, 'fs', [(i, i ^ far) for i in range(size)])  131 us
    all_to_all x2, blocking collectives, relayout(): lax.all_to_all(down_part, 'fs', split_axis=0, concat_axis=1, tiled=True)  121 us
    reduce_scatter x1, waiting for transfers between devices, shards(): lax.psum_scatter(projector(hidden_second, down_flat_two), 'fs', scatter_d...  82.8 us
    all_to_all x1, blocking collectives, relayout(): lax.all_to_all(gate_part, 'fs', split_axis=0, concat_axis=1, tiled=True)  28.1 us
    all_to_all x1, blocking collectives, relayout(): lax.all_to_all(up_part, 'fs', split_axis=0, concat_axis=1, tiled=True)  22.3 us
    unnamed x42, local copies, waits for them, and re-layouts  20.3 us
  transfers between devices with their start and end apart: 13, of which 7 were waited for; matrix products, arithmetic and copies ran while one was open for 6% of the time, Pallas kernels for 0%

profile of v1, /device:TPU:0, one launch (start us, length us, event | category | flops | bytes accessed | tf_op | source)
XLA Modules:
  0.0 488.8 jit_solution(699186305656697307)
XLA Ops:
  7.2 1.8 copy.40
  9.0 1.8 copy.42
  10.8 1.1 multiply_convert_fusion.3
  11.9 28.1 %all_to_all.96 = bf16[16,176,128]{2,1,0:T(8,128)(2,1)S(1)} all-to-all(bf16[16,176,128]{2,1,0:T(8,128)(2,1)S(1)} %bitcast.56), channel_id=1, replica_groups=mesh['fs'=16,'tp'=2] {'fs'}, dimensions={0} | all-to-all | bytes 1441792 | tf_op jit(solution)/shard_map/all_to_all | solution.py:19
  40.3 1.2 broadcast_in_dim.27
  41.5 22.3 %all_to_all.97 = bf16[16,176,128]{2,1,0:T(8,128)(2,1)S(1)} all-to-all(bf16[16,176,128]{2,1,0:T(8,128)(2,1)S(1)} %bitcast.55), channel_id=1, replica_groups=mesh['fs'=16,'tp'=2] {'fs'}, dimensions={0} | all-to-all | bytes 1441792 | tf_op jit(solution)/shard_map/all_to_all | solution.py:20
  64.0 1.2 broadcast_in_dim.28
  66.0 22.3 %all_to_all.98 = bf16[16,176,128]{2,1,0:T(8,128)(2,1)S(1)} all-to-all(bf16[16,176,128]{2,1,0:T(8,128)(2,1)S(1)} %bitcast.63), channel_id=1, replica_groups=mesh['fs'=16,'tp'=2] {'fs'}, dimensions={0} | all-to-all | bytes 1441792 | tf_op jit(solution)/shard_map/all_to_all | solution.py:21
  88.5 1.2 broadcast_in_dim.29
  90.1 2.0 fusion.12
  92.1 5.0 %all-gather.11.cloned.1.call-done = bf16[2,176,2048]{2,1,0:T(8,128)(2,1)} async-done(((bf16[1,176,2048]{2,1,0:T(8,128)(2,1)}), bf16[2,176,2048]{2,1,0:T(8,128)(2,1)}) %all-gather.11.cloned.1.call-update) | async-done | bytes 1441808 | tf_op jit(solution)/shard_map/all_gather | solution.py:26
  97.1 3.9 fusion.8
  101.0 1.8 collective-permute-start
  102.8 46.1 %collective-permute-done = f32[256,2048]{1,0:T(8,128)S(1)} collective-permute-done((f32[256,2048]{1,0:T(8,128)S(1)}, f32[256,2048]{1,0:T(8,128)S(1)}, u32[]{:S(2)}, u32[]{:S(2)}) %collective-permute-start) | collective-permute-done | bytes 2097184 | tf_op jit(solution)/shard_map/ppermute | solution.py:72
  148.9 1.9 add.48
  150.8 1.8 collective-permute-start.1
  152.6 1.8 copy.46
  154.4 2.9 copy.48
  157.3 2.7 multiply_convert_fusion.1
  160.0 5.7 %all-to-all-start.4 = ((bf16[16,176,128]{2,1,0:T(8,128)(2,1)}), bf16[16,176,128]{2,1,0:T(8,128)(2,1)S(1)}, u32[]{:S(2)}, u32[]{:S(2)}) async-start(bf16[16,176,128]{2,1,0:T(8,128)(2,1)} %bitcast.54), calls=%async_computation.4 | async-start | bytes 1441792 | tf_op jit(solution)/shard_map/all_to_all | solution.py:20
  165.8 39.4 %collective-permute-done.1 = f32[256,2048]{1,0:T(8,128)} collective-permute-done((f32[256,2048]{1,0:T(8,128)S(1)}, f32[256,2048]{1,0:T(8,128)}, u32[]{:S(2)}, u32[]{:S(2)}) %collective-permute-start.1) | collective-permute-done | bytes 2097184 | tf_op jit(solution)/shard_map/ppermute | solution.py:72
  205.2 2.5 add.49
  207.7 1.8 collective-permute-start.2
  209.7 1.2 broadcast_in_dim.31
  210.9 5.6 %all-to-all-start.3 = ((bf16[16,176,128]{2,1,0:T(8,128)(2,1)}), bf16[16,176,128]{2,1,0:T(8,128)(2,1)S(1)}, u32[]{:S(2)}, u32[]{:S(2)}) async-start(bf16[16,176,128]{2,1,0:T(8,128)(2,1)} %bitcast.15), calls=%async_computation.3 | async-start | bytes 1441792 | tf_op jit(solution)/shard_map/all_to_all | solution.py:19
  216.5 45.6 %collective-permute-done.2 = f32[256,2048]{1,0:T(8,128)} collective-permute-done((f32[256,2048]{1,0:T(8,128)S(1)}, f32[256,2048]{1,0:T(8,128)}, u32[]{:S(2)}, u32[]{:S(2)}) %collective-permute-start.2) | collective-permute-done | bytes 2097184 | tf_op jit(solution)/shard_map/ppermute | solution.py:72
  262.2 3.2 add.50
  265.4 5.5 %all-to-all-done.3 = bf16[16,176,128]{2,1,0:T(8,128)(2,1)S(1)} async-done(((bf16[16,176,128]{2,1,0:T(8,128)(2,1)}), bf16[16,176,128]{2,1,0:T(8,128)(2,1)S(1)}, u32[]{:S(2)}, u32[]{:S(2)}) %all-to-all-start.3) | async-done | bytes 720928 | tf_op jit(solution)/shard_map/all_to_all | solution.py:19
  271.1 1.2 broadcast_in_dim.30
  273.1 98.8 %all_to_all.99 = bf16[16,176,128]{2,1,0:T(8,128)(2,1)S(1)} all-to-all(bf16[16,176,128]{2,1,0:T(8,128)(2,1)S(1)} %bitcast.64), channel_id=1, replica_groups=mesh['fs'=16,'tp'=2] {'fs'}, dimensions={0} | all-to-all | bytes 1441792 | tf_op jit(solution)/shard_map/all_to_all | solution.py:21
  372.1 1.2 broadcast_in_dim.32
  373.6 2.8 fusion.2
  376.4 2.0 fusion.14
  378.4 3.2 all-gather.17.cloned.1.call-done
  381.7 5.3 %fusion.23 = f32[256,2048]{1,0:T(8,128)} fusion(bf16[352,2048]{1,0:T(8,128)(2,1)} %bitcast.70, f32[256,352]{0,1:T(8,128)S(1)} %fusion.14, bf16[352,2048]{1,0:T(8,128)(2,1)} %bitcast.69, bf16[256,2048]{1,0:T(8,128)(2,1)S(1)} %get-tuple-element.8, f32[256]{0:T(256)S(1)} %add_rsqrt_fusion), kind=kOutput, calls=%fused_computation.28 | convolution fusion | flops 740311040 | bytes 6390784 | tf_op jit(solution)/shard_map/dot_general | solution.py:39
  387.0 82.8 %reduce-scatter.2.cloned.1.call-done = f32[16,2048]{1,0:T(8,128)} async-done(((f32[256,2048]{1,0:T(8,128)}), f32[16,2048]{1,0:T(8,128)}) %reduce-scatter.2.cloned.1.call-update) | async-done | bytes 131088 | tf_op jit(solution)/shard_map/reduce_scatter | solution.py:78
  469.8 1.6 fusion.30
  471.4 1.1 copy.58
  472.5 0.8 copy-done.8
  473.3 1.1 copy.59
  474.4 0.8 copy-done.9
  475.2 1.1 copy.60
  476.3 0.8 copy-done.11
  477.1 1.1 copy.61
  478.2 0.8 copy-done.10
  478.9 1.1 copy.62
  480.0 0.8 copy-done.12
  480.8 1.1 copy.63
  (57 shorter events, 3.6 us)
Async XLA Ops:
  7.2 82.9 %all-gather.7.cloned.1.call-start = ((), (), s32[]{:S(2)}) async-start(), calls=%async_computation.7 | async-start | bytes 2162688 | tf_op jit(solution)/shard_map/all_gather | solution.py:24
  9.0 1.8 copy-start.13
  40.2 1.3 copy-start.3
  41.4 50.7 %all-gather.9.cloned.1.call-start = ((), (), s32[]{:S(2)}) async-start(), calls=%async_computation.8 | async-start | bytes 2162688 | tf_op jit(solution)/shard_map/all_gather | solution.py:25
  64.0 1.6 copy-start.5
  65.2 31.9 %all-gather.11.cloned.1.call-start = ((), (), s32[]{:S(2)}) async-start(), calls=%async_computation.9 | async-start | bytes 2162688 | tf_op jit(solution)/shard_map/all_gather | solution.py:26
  88.5 1.2 copy-start.1
  101.0 1.8 copy-start.4
  101.0 47.9 %collective-permute-start = (f32[256,2048]{1,0:T(8,128)S(1)}, f32[256,2048]{1,0:T(8,128)S(1)}, u32[]{:S(2)}, u32[]{:S(2)}) collective-permute-start(f32[256,2048]{1,0:T(8,128)S(1)} %fusion.8), channel_id=1, source_target_pairs={{0,2},{2,0},{4,6},{6,4},{8,10},{10,8},{12,14},{14,12},{16,18},{18,... | collective-permute-start | bytes 6291464 | tf_op jit(solution)/shard_map/ppermute | solution.py:72
  150.8 3.6 copy-start
  150.8 54.4 %collective-permute-start.1 = (f32[256,2048]{1,0:T(8,128)S(1)}, f32[256,2048]{1,0:T(8,128)}, u32[]{:S(2)}, u32[]{:S(2)}) collective-permute-start(f32[256,2048]{1,0:T(8,128)S(1)} %add.48), channel_id=1, source_target_pairs={{0,4},{2,6},{4,0},{6,2},{8,12},{10,14},{12,8},{14,10},{16,20},{18,... | collective-permute-start | bytes 6291464 | tf_op jit(solution)/shard_map/ppermute | solution.py:72
  154.4 2.9 copy-start.14
  160.0 49.5 %all-to-all-start.4 = ((bf16[16,176,128]{2,1,0:T(8,128)(2,1)}), bf16[16,176,128]{2,1,0:T(8,128)(2,1)S(1)}, u32[]{:S(2)}, u32[]{:S(2)}) async-start(bf16[16,176,128]{2,1,0:T(8,128)(2,1)} %bitcast.54), calls=%async_computation.4 | async-start | bytes 1441792 | tf_op jit(solution)/shard_map/all_to_all | solution.py:20
  165.7 210.7 %all-gather.15.cloned.1.call-start = ((), (), s32[]{:S(2)}) async-start(), calls=%async_computation.11 | async-start | bytes 2162688 | tf_op jit(solution)/shard_map/all_gather | solution.py:25
  207.7 54.5 %collective-permute-start.2 = (f32[256,2048]{1,0:T(8,128)S(1)}, f32[256,2048]{1,0:T(8,128)}, u32[]{:S(2)}, u32[]{:S(2)}) collective-permute-start(f32[256,2048]{1,0:T(8,128)S(1)} %add.49), channel_id=1, source_target_pairs={{0,8},{2,10},{4,12},{6,14},{8,0},{10,2},{12,4},{14,6},{16,24},{18,... | collective-permute-start | bytes 6291464 | tf_op jit(solution)/shard_map/ppermute | solution.py:72
  210.9 60.1 %all-to-all-start.3 = ((bf16[16,176,128]{2,1,0:T(8,128)(2,1)}), bf16[16,176,128]{2,1,0:T(8,128)(2,1)S(1)}, u32[]{:S(2)}, u32[]{:S(2)}) async-start(bf16[16,176,128]{2,1,0:T(8,128)(2,1)} %bitcast.15), calls=%async_computation.3 | async-start | bytes 1441792 | tf_op jit(solution)/shard_map/all_to_all | solution.py:19
  216.5 162.0 %all-gather.13.cloned.1.call-start = ((), (), s32[]{:S(2)}) async-start(), calls=%async_computation.10 | async-start | bytes 2162688 | tf_op jit(solution)/shard_map/all_gather | solution.py:24
  265.4 108.2 %collective-permute-start.3 = (f32[256,2048]{1,0:T(8,128)}, f32[256,2048]{1,0:T(8,128)}, u32[]{:S(2)}, u32[]{:S(2)}) collective-permute-start(f32[256,2048]{1,0:T(8,128)} %add.50), channel_id=1, source_target_pairs={{0,16},{2,18},{4,20},{6,22},{8,24},{10,26},{12,28},{14,30},{16,0},... | collective-permute-start | bytes 6291464 | tf_op jit(solution)/shard_map/ppermute | solution.py:72
  271.1 1.6 copy-start.6
  272.3 109.4 %all-gather.17.cloned.1.call-start = ((), (), s32[]{:S(2)}) async-start(), calls=%async_computation.12 | async-start | bytes 2162688 | tf_op jit(solution)/shard_map/all_gather | solution.py:26
  372.1 1.4 copy-start.2
  373.3 96.5 %reduce-scatter.2.cloned.1.call-start = ((), (), s32[]{:S(2)}) async-start(), calls=%async_computation.13 | async-start | bytes 2228224 | tf_op jit(solution)/shard_map/reduce_scatter | solution.py:78
  387.0 84.4 %copy-start.7 = (bf16[2,176,2048]{2,1,0:T(8,128)(2,1)S(1)}, bf16[2,176,2048]{2,1,0:T(8,128)(2,1)}, u32[]{:S(2)}) copy-start(bf16[2,176,2048]{2,1,0:T(8,128)(2,1)} %all-gather.7.cloned.1.call-done) | copy-start | bytes 4325380
  471.4 1.9 copy-start.8
  473.3 1.9 copy-start.9
  475.2 1.9 copy-start.11
  477.1 1.9 copy-start.10
  478.9 1.9 copy-start.12
Sparse Core Ops, SparseCore 0:
  41.6 7.2 all-gather.6
  65.3 7.2 all-gather.8
  89.8 7.2 all-gather.10
  211.0 9.5 all-gather.14
  272.4 7.6 all-gather.12
  373.4 8.2 all-gather.16
  387.1 82.6 reduce-scatter.1
